TPU v7x, 32 devices: a whole 2x2x4 slice. The times are simulated.
32 devices in a mesh: kv: 16 (over z, y, x), tp: 2 (over core).
Axes of the slice: x: 2, y: 2, z: 4, core: 2. Of those that a mesh axis runs over, the one named last changes fastest.
Arguments:
- queries: bfloat16 [2048, 1024], P('kv', 'tp'), may hold values from -4 to 4
- keys: bfloat16 [2048, 1024], P('kv', 'tp'), may hold values from -4 to 4
- values: bfloat16 [2048, 1024], P('kv', 'tp'), may hold values from -4 to 4
- cotangent: bfloat16 [2048, 1024], P('kv', 'tp'), may hold values from -4 to 4
- log_sum: float32 [16, 2048], P('tp', 'kv'), may hold values from 4.5 to 7.5
- chosen: int32 [16, 64, 12], P('tp'), may hold values from 0 to 63, as said below
- normed_input: bfloat16 [2048, 2048], P('kv', 'tp'), may hold values from -0.125 to 0.125
Outputs:
- grad_queries: bfloat16 [2048, 1024], P('kv', 'tp')
- grad_keys: bfloat16 [2048, 1024], P('kv', 'tp')
- grad_values: bfloat16 [2048, 1024], P('kv', 'tp')
- grad_weight: float32 [2048, 1024], P('kv', 'tp')
Inputs may be any that keep to these rules, and one draw needn't show every extreme that they name: `chosen`: for each head, the distinct blocks below their own query block that the query blocks of one device's 128 positions choose include at most 1 block of any one device's span of 128 positions, and exactly 1 for some pairs of devices. Within one list the entries below the query block's own index are distinct.
All inputs are finite; a program needn't handle non-finite values.
Results may differ from a plain program's by a relative error of at most 0.0085.
Values may be sent and summed in bfloat16 or wider, within the bound.
A program may use at most 64 MiB of HBM per device.

v0:
```python
import jax
import jax.numpy as jnp
from jax import lax
from jax.sharding import PartitionSpec as P

HD = 64
BLK = 32
SEL = 12
MOST = 1


MASKED = -1e30


def slot_picks(needed):
    span_width = needed.shape[-1]
    counted = needed.astype(jnp.int32)
    before = jnp.cumsum(counted, axis=-1) - counted
    places = jnp.arange(span_width, dtype=jnp.int32)
    picked, present = ([], [])
    hitting = needed & (before == 0)
    present.append(jnp.any(hitting, axis=-1))
    picked.append(jnp.sum(jnp.where(hitting, places, 0), axis=-1))
    return (jnp.stack(picked, axis=-1), jnp.stack(present, axis=-1))


def to_blocks(row_block, tok_rows, head_count):
    shards = row_block.shape[0] // tok_rows
    shaped = row_block.reshape(shards, tok_rows // BLK, BLK, head_count, HD).transpose(
        0, 3, 1, 2, 4
    )
    return shaped.reshape(shards * head_count * (tok_rows // BLK), BLK * HD)


def heads_from(row_block, head_count):
    blocks_dev = row_block.shape[0] // BLK
    return row_block.reshape(blocks_dev, BLK, head_count, HD).transpose(2, 0, 1, 3)


def back_rows(blocked):
    head_count, blocks_dev = (blocked.shape[0], blocked.shape[1])
    return blocked.transpose(1, 2, 0, 3).reshape(blocks_dev * BLK, head_count * HD)


def body(queries, keys, values, cotangent, log_sum, chosen, normed_input):
    tok_rows = queries.shape[0]
    head_count = log_sum.shape[0]
    blocks_dev = tok_rows // BLK
    devices = lax.axis_size("kv")
    my_index = lax.axis_index("kv")
    block_total = chosen.shape[1]
    tile_size = BLK * HD
    score_scale = HD ** (-0.5)
    places = jnp.arange(blocks_dev, dtype=jnp.int32)
    own_ids = my_index * blocks_dev + places
    my_lists = lax.dynamic_slice_in_dim(chosen, my_index * blocks_dev, blocks_dev, 1)
    usable = my_lists < own_ids[None, :, None]
    every_block = jnp.arange(block_total, dtype=jnp.int32)
    need_here = jnp.any((my_lists[..., None] == every_block) & usable[..., None], axis=(1, 2))
    req_picked, req_present = slot_picks(need_here.reshape(head_count, devices, blocks_dev))
    grouped = chosen.reshape(head_count, devices, blocks_dev, SEL)
    row_ids = every_block.reshape(devices, blocks_dev)
    usable_all = grouped < row_ids[None, :, :, None]
    need_there = jnp.any((grouped[..., None] == own_ids) & usable_all[..., None], axis=(2, 3))
    own_picked, own_present = slot_picks(need_there)
    own_picked = own_picked.transpose(1, 0, 2)
    own_present = own_present.transpose(1, 0, 2)
    head_base = (jnp.arange(head_count, dtype=jnp.int32) * blocks_dev)[None, :, None]
    send_ids = (head_base + own_picked).reshape(-1)
    key_send = jnp.take(to_blocks(keys, tok_rows, head_count), send_ids, axis=0).reshape(
        devices, head_count, MOST, tile_size
    )
    value_send = jnp.take(to_blocks(values, tok_rows, head_count), send_ids, axis=0).reshape(
        devices, head_count, MOST, tile_size
    )
    key_tiles, value_tiles = (
        lax.all_to_all(key_send, "kv", split_axis=0, concat_axis=0, tiled=True),
        lax.all_to_all(value_send, "kv", split_axis=0, concat_axis=0, tiled=True),
    )
    owners = my_lists // blocks_dev
    local_ids = my_lists % blocks_dev
    head_ids = jnp.arange(head_count, dtype=jnp.int32)[:, None, None]
    rows_at = (head_ids * devices + owners).reshape(-1)
    slot_at = jnp.take(req_picked.reshape(head_count * devices, MOST), rows_at, axis=0).reshape(
        head_count, blocks_dev, SEL, MOST
    )
    slot_live = jnp.take(req_present.reshape(head_count * devices, MOST), rows_at, axis=0).reshape(
        head_count, blocks_dev, SEL, MOST
    )
    matches = (slot_at == local_ids[..., None]) & slot_live
    slot_of = jnp.sum(jnp.where(matches, jnp.arange(MOST, dtype=jnp.int32), 0), axis=-1)
    tile_ids = jnp.where(usable, (owners * head_count + head_ids) * MOST + slot_of, 0).reshape(-1)
    sel_keys = jnp.take(key_tiles.reshape(-1, tile_size), tile_ids, axis=0).reshape(
        head_count, blocks_dev, SEL * BLK, HD
    )
    sel_values = jnp.take(value_tiles.reshape(-1, tile_size), tile_ids, axis=0).reshape(
        head_count, blocks_dev, SEL * BLK, HD
    )
    keys_all = jnp.concatenate([sel_keys, heads_from(keys, head_count)], axis=2)
    values_all = jnp.concatenate([sel_values, heads_from(values, head_count)], axis=2)
    causal = jnp.arange(BLK)[:, None] >= jnp.arange(BLK)[None, :]
    sel_mask = jnp.broadcast_to(
        jnp.repeat(usable, BLK, axis=2)[:, :, None, :], (head_count, blocks_dev, BLK, SEL * BLK)
    )
    allowed = jnp.concatenate(
        [sel_mask, jnp.broadcast_to(causal, (head_count, blocks_dev, BLK, BLK))], axis=3
    )
    q_blocks = heads_from(queries, head_count)
    g_blocks = heads_from(cotangent, head_count)
    log_rows = log_sum.reshape(head_count, blocks_dev, BLK)[..., None]
    scores = (
        jnp.einsum("hiqd,hikd->hiqk", q_blocks, keys_all, preferred_element_type=jnp.float32)
        * score_scale
    )
    weights = jnp.exp(jnp.where(allowed, scores - log_rows, MASKED))
    value_dots = jnp.einsum(
        "hiqd,hikd->hiqk", g_blocks, values_all, preferred_element_type=jnp.float32
    )
    row_delta = jnp.sum(weights * value_dots, axis=-1, keepdims=True)
    score_grad = (weights * (value_dots - row_delta)).astype(jnp.bfloat16)
    weights_low = weights.astype(jnp.bfloat16)
    query_grad = (
        jnp.einsum("hiqk,hikd->hiqd", score_grad, keys_all, preferred_element_type=jnp.float32)
        * score_scale
    )
    key_grad = (
        jnp.einsum("hiqk,hiqd->hikd", score_grad, q_blocks, preferred_element_type=jnp.float32)
        * score_scale
    )
    value_grad = jnp.einsum(
        "hiqk,hiqd->hikd", weights_low, g_blocks, preferred_element_type=jnp.float32
    )
    grad_queries = back_rows(query_grad).astype(jnp.bfloat16)

    def to_slots(gradient):
        chosen_part = gradient[:, :, : SEL * BLK].reshape(-1, tile_size)
        slotted = jax.ops.segment_sum(
            chosen_part, tile_ids, num_segments=devices * head_count * MOST
        )
        return slotted.reshape(devices, head_count, MOST, tile_size)

    back_keys, back_values = (
        lax.all_to_all(to_slots(key_grad), "kv", split_axis=0, concat_axis=0, tiled=True),
        lax.all_to_all(to_slots(value_grad), "kv", split_axis=0, concat_axis=0, tiled=True),
    )
    land_ids = jnp.where(own_present, head_base + own_picked, head_count * blocks_dev).reshape(-1)

    def settle(returned, gradient):
        flat_tiles = returned.reshape(-1, tile_size)
        targets = (
            jnp.arange(head_count * blocks_dev, dtype=jnp.int32)[:, None] == land_ids[None, :]
        ).astype(jnp.float32)
        landed = jnp.dot(
            targets, flat_tiles, precision=lax.Precision.HIGHEST, preferred_element_type=jnp.float32
        )
        summed = landed.reshape(head_count, blocks_dev, BLK, HD) + gradient[:, :, SEL * BLK :]
        return back_rows(summed).astype(jnp.bfloat16)

    grad_keys = settle(back_keys, key_grad)
    grad_values = settle(back_values, value_grad)
    whole_input = lax.all_gather(normed_input, "tp", axis=1, tiled=True)
    grad_weight = lax.psum_scatter(
        lax.dot_general(
            whole_input, grad_queries, (((0,), (0,)), ((), ())), preferred_element_type=jnp.float32
        ),
        "kv",
        scatter_dimension=0,
        tiled=True,
    )
    return (grad_queries, grad_keys, grad_values, grad_weight)


def solution(mesh):
    in_specs = (
        P("kv", "tp"),
        P("kv", "tp"),
        P("kv", "tp"),
        P("kv", "tp"),
        P("tp", "kv"),
        P("tp", None, None),
        P("kv", "tp"),
    )
    out_specs = (P("kv", "tp"), P("kv", "tp"), P("kv", "tp"), P("kv", "tp"))
    return jax.shard_map(body, mesh=mesh, in_specs=in_specs, out_specs=out_specs, check_vma=False)
```

profile of v0, /device:TPU:0, one launch (start us, length us, event | category | flops | bytes accessed | tf_op | source)
XLA Modules:
  0.0 212.2 jit_solution(2276714439298911949)
XLA Ops:
  7.2 1.0 copy.82
  8.2 0.3 copy.83
  8.6 0.3 copy.84
  9.0 0.2 and_reduce_fusion
  9.5 1.1 reshape.197
  10.6 0.3 reshape.198
  10.9 0.2 reshape.188
  11.2 0.3 reshape.189
  11.4 0.9 gather_fusion.2
  12.4 0.9 gather_fusion
  13.3 1.1 select_bitcast_fusion
  14.5 8.5 %all-to-all-start.1 = ((bf16[16,8,1,2048]{3,1,2,0:T(8,128)(2,1)}), bf16[16,8,1,2048]{3,1,2,0:T(8,128)(2,1)S(1)}, u32[]{:S(2)}, u32[]{:S(2)}) async-start(bf16[16,8,1,2048]{3,1,2,0:T(8,128)(2,1)} %get-tuple-element.28), calls=%async_computation.1 | async-start | bytes 1048576 | tf_op jit(solution)/shard_map/all_to_all | solution.py:78
  23.4 1.1 copy.93
  24.5 13.6 %all-to-all-done.1 = bf16[16,8,1,2048]{3,1,2,0:T(8,128)(2,1)S(1)} async-done(((bf16[16,8,1,2048]{3,1,2,0:T(8,128)(2,1)}), bf16[16,8,1,2048]{3,1,2,0:T(8,128)(2,1)S(1)}, u32[]{:S(2)}, u32[]{:S(2)}) %all-to-all-start.1) | async-done | bytes 524320 | tf_op jit(solution)/shard_map/all_to_all | solution.py:78
  38.0 3.9 %all-to-all-start = ((bf16[16,8,1,2048]{3,1,2,0:T(8,128)(2,1)}), bf16[16,8,1,2048]{3,1,2,0:T(8,128)(2,1)S(1)}, u32[]{:S(2)}, u32[]{:S(2)}) async-start(bf16[16,8,1,2048]{3,1,2,0:T(8,128)(2,1)} %get-tuple-element.29), calls=%async_computation | async-start | bytes 1048576 | tf_op jit(solution)/shard_map/all_to_all | solution.py:77
  42.7 1.1 copy.88
  43.8 0.9 reshape.196
  45.2 2.5 %all_gather.3 = bf16[128,2048]{1,0:T(8,128)(2,1)} all-gather(bf16[128,1024]{1,0:T(8,128)(2,1)S(1)} %copy-done.12), channel_id=1, replica_groups=mesh['kv'=16,'tp'=2] {'tp'}, dimensions={1}, use_global_device_ids=true | all-gather | bytes 786432 | tf_op jit(solution)/shard_map/all_gather | solution.py:161
  47.7 2.4 %gather_fusion.3 = bf16[384,2048]{1,0:T(8,128)(2,1)S(1)} fusion(bf16[128,2048]{1,0:T(8,128)(2,1)S(1)} %bitcast.115, s32[1024]{0:T(1024)S(1)} %pad_clamp_fusion), kind=kCustom, calls=%fused_computation.3.clone | custom fusion | bytes 3147264 | tf_op jit(solution)/shard_map/jit(_take)/gather | solution.py:96
  50.1 6.3 %all-to-all-done = bf16[16,8,1,2048]{3,1,2,0:T(8,128)(2,1)S(1)} async-done(((bf16[16,8,1,2048]{3,1,2,0:T(8,128)(2,1)}), bf16[16,8,1,2048]{3,1,2,0:T(8,128)(2,1)S(1)}, u32[]{:S(2)}, u32[]{:S(2)}) %all-to-all-start) | async-done | bytes 524320 | tf_op jit(solution)/shard_map/all_to_all | solution.py:77
  56.4 3.1 %gather_fusion.1 = bf16[384,2048]{1,0:T(8,128)(2,1)} fusion(bf16[128,2048]{1,0:T(8,128)(2,1)S(1)} %bitcast.116, s32[1024]{0:T(1024)S(1)} %pad_clamp_fusion), kind=kCustom, calls=%fused_computation.1.clone | custom fusion | bytes 3147264 | tf_op jit(solution)/shard_map/jit(_take)/gather | solution.py:93
  59.6 3.4 %broadcast_select_fusion = (bf16[384,2048]{1,0:T(8,128)(2,1)}, bf16[384,2048]{1,0:T(8,128)(2,1)}) fusion(bf16[384,2048]{1,0:T(8,128)(2,1)S(1)} %gather_fusion.3, pred[384]{0:T(512)(128)(4,1)S(1)} %compare_and_fusion, bf16[384,2048]{1,0:T(8,128)(2,1)} %gather_fusion.1), kind=kLoop, calls=%fused_computation.20 | loop fusion | flops 1572864 | bytes 6291840 | tf_op jit(solution)/shard_map/jit(_take)/select_n | solution.py:96
  62.9 4.6 %reshape.201 = bf16[8,4,384,64]{3,2,1,0:T(8,128)(2,1)S(1)} reshape(bf16[384,2048]{1,0:T(8,128)(2,1)} %get-tuple-element.26) | data formatting | bytes 3145728 | tf_op jit(solution)/shard_map/reshape | solution.py:96
  67.5 2.5 %copy.94 = bf16[8,4,384,64]{2,3,1,0:T(8,128)(2,1)} copy(bf16[8,4,384,64]{3,2,1,0:T(8,128)(2,1)S(1)} %reshape.201) | data formatting | bytes 3145728 | tf_op jit(solution)/shard_map/reshape | solution.py:96
  70.0 4.6 %reshape.194 = bf16[8,4,384,64]{3,2,1,0:T(8,128)(2,1)S(1)} reshape(bf16[384,2048]{1,0:T(8,128)(2,1)} %get-tuple-element.27) | data formatting | bytes 3145728 | tf_op jit(solution)/shard_map/reshape | solution.py:93
  74.6 2.5 %copy.89 = bf16[8,4,384,64]{2,3,1,0:T(8,128)(2,1)} copy(bf16[8,4,384,64]{3,2,1,0:T(8,128)(2,1)S(1)} %reshape.194) | data formatting | bytes 3145728 | tf_op jit(solution)/shard_map/reshape | solution.py:93
  77.1 2.1 %fusion = f32[8,4,416,32]{2,3,1,0:T(8,128)S(1)} fusion(bf16[8,4,32,64]{2,3,1,0:T(8,128)(2,1)} %bitcast.122, bf16[8,4,384,64]{2,3,1,0:T(8,128)(2,1)} %copy.94, bf16[4,32,8,64]{3,2,1,0:T(8,128)(2,1)S(1)} %reshape.203), kind=kOutput, calls=%fused_computation.9 | convolution fusion | flops 57933824 | bytes 3538944 | tf_op jit(solution)/shard_map/hiqd,hikd->hiqk/dot_general | solution.py:116
  79.4 1.2 fusion.4
  80.6 0.3 fusion.6
  80.9 1.0 copy-done.2
  81.9 0.7 fusion.11
  82.8 0.2 convert_element_type.43
  83.0 2.8 %convolution_bitcast_fusion = f32[2048,512]{0,1:T(8,128)} fusion(bf16[128,512]{1,0:T(8,128)(2,1)S(1)} %convert_element_type.43, bf16[128,2048]{1,0:T(8,128)(2,1)S(1)} %copy-done.4), kind=kOutput, calls=%fused_computation.6 | convolution fusion | flops 268435456 | bytes 4849664 | tf_op jit(solution)/shard_map/dot_general | solution.py:163
  85.8 0.9 copy-done.7
  86.7 0.7 convolution_multiply_fusion
  87.5 2.1 copy-done.1
  89.6 0.4 slice.24
  89.9 4.2 %copy.98 = f32[8,4,384,64]{3,2,1,0:T(8,128)} copy(f32[8,4,384,64]{2,3,1,0:T(8,128)S(1)} %slice.24) | data formatting | bytes 6291456 | tf_op jit(solution)/shard_map/slice | solution.py:136
  94.2 6.4 %reshape.246 = f32[384,2048]{1,0:T(8,128)} reshape(f32[8,4,384,64]{3,2,1,0:T(8,128)} %copy.98) | data formatting | bytes 6291456 | tf_op jit(solution)/shard_map/reshape | solution.py:136
  100.6 8.0 %scatter_custom_fusion = f32[128,2048]{1,0:T(8,128)} fusion(s32[384]{0:T(512)S(1)} %reshape.193, f32[384,2048]{1,0:T(8,128)} %reshape.246, f32[]{:T(128)} %constant.106.clone.1), kind=kCustom, calls=%fused_computation.42 | custom fusion | flops 786432 | bytes 1049088 | tf_op jit(solution)/shard_map/scatter-add | solution.py:137
  108.5 4.3 %all-to-all-start.2 = ((f32[16,8,1,2048]{3,1,2,0:T(8,128)}), f32[16,8,1,2048]{3,1,2,0:T(8,128)}, u32[]{:S(2)}, u32[]{:S(2)}) async-start(f32[16,8,1,2048]{3,1,2,0:T(8,128)} %bitcast.23), calls=%async_computation.2 | async-start | bytes 2097152 | tf_op jit(solution)/shard_map/all_to_all | solution.py:143
  112.9 0.8 fusion.16
  113.7 2.0 copy-done
  115.6 0.4 slice.26
  116.0 4.2 %copy.103 = f32[8,4,384,64]{3,2,1,0:T(8,128)} copy(f32[8,4,384,64]{2,3,1,0:T(8,128)S(1)} %slice.26) | data formatting | bytes 6291456 | tf_op jit(solution)/shard_map/slice | solution.py:136
  120.2 5.0 %reshape.254 = f32[384,2048]{1,0:T(8,128)S(1)} reshape(f32[8,4,384,64]{3,2,1,0:T(8,128)} %copy.103) | data formatting | bytes 6291456 | tf_op jit(solution)/shard_map/reshape | solution.py:136
  125.2 6.3 %scatter_custom_fusion.1 = f32[128,2048]{1,0:T(8,128)} fusion(s32[384]{0:T(512)S(1)} %reshape.193, f32[384,2048]{1,0:T(8,128)S(1)} %reshape.254, f32[]{:T(128)} %constant.106.clone.1), kind=kCustom, calls=%fused_computation.40 | custom fusion | flops 786432 | bytes 1048580 | tf_op jit(solution)/shard_map/scatter-add | solution.py:137
  131.5 11.6 %all-to-all-done.2 = f32[16,8,1,2048]{3,1,2,0:T(8,128)} async-done(((f32[16,8,1,2048]{3,1,2,0:T(8,128)}), f32[16,8,1,2048]{3,1,2,0:T(8,128)}, u32[]{:S(2)}, u32[]{:S(2)}) %all-to-all-start.2) | async-done | bytes 1048608 | tf_op jit(solution)/shard_map/all_to_all | solution.py:143
  143.1 10.4 %all-to-all-start.3 = ((f32[16,8,1,2048]{3,1,2,0:T(8,128)}), f32[16,8,1,2048]{3,1,2,0:T(8,128)S(1)}, u32[]{:S(2)}, u32[]{:S(2)}) async-start(f32[16,8,1,2048]{3,1,2,0:T(8,128)} %bitcast.31), calls=%async_computation.3 | async-start | bytes 2097152 | tf_op jit(solution)/shard_map/all_to_all | solution.py:144
  153.7 1.6 copy.100
  155.2 1.6 fusion.40
  156.8 0.4 copy.101
  157.2 1.4 fusion.18
  158.6 0.2 copy.102
  158.8 0.9 convert_element_type.46
  159.7 24.2 %all-to-all-done.3 = f32[16,8,1,2048]{3,1,2,0:T(8,128)S(1)} async-done(((f32[16,8,1,2048]{3,1,2,0:T(8,128)}), f32[16,8,1,2048]{3,1,2,0:T(8,128)S(1)}, u32[]{:S(2)}, u32[]{:S(2)}) %all-to-all-start.3) | async-done | bytes 1048608 | tf_op jit(solution)/shard_map/all_to_all | solution.py:144
  183.9 0.3 copy.105
  184.2 1.6 fusion.38
  185.8 0.4 copy.106
  186.2 1.4 fusion.19
  187.6 0.2 copy.107
  187.8 0.9 convert_element_type.50
  188.7 14.9 %reduce-scatter.2.cloned.1.call-done = f32[128,512]{0,1:T(8,128)} async-done(((f32[2048,512]{0,1:T(8,128)}), f32[128,512]{0,1:T(8,128)}) %reduce-scatter.2.cloned.1.call-update) | async-done | bytes 262160 | tf_op jit(solution)/shard_map/reduce_scatter | solution.py:162
  203.6 1.8 copy.108
  (67 shorter events, 2.6 us)
Async XLA Ops:
  7.2 3.8 %copy-start.9 = (bf16[128,512]{1,0:T(8,128)(2,1)S(1)}, bf16[128,512]{1,0:T(8,128)(2,1)}, u32[]{:S(2)}) copy-start(bf16[128,512]{1,0:T(8,128)(2,1)} %param.12) | copy-start | bytes 393220
  13.3 9.6 %copy-start.8 = (bf16[128,512]{1,0:T(8,128)(2,1)S(1)}, bf16[128,512]{1,0:T(8,128)(2,1)}, u32[]{:S(2)}) copy-start(bf16[128,512]{1,0:T(8,128)(2,1)} %param.13) | copy-start | bytes 393220
  14.5 27.6 %copy-start.13 = (s32[8,64,12]{1,0,2:T(8,128)S(1)}, s32[8,64,12]{1,0,2:T(8,128)}, u32[]{:S(2)}) copy-start(s32[8,64,12]{1,0,2:T(8,128)} %param.16) | copy-start | bytes 73732
  14.5 28.0 %copy-start.14 = (bf16[128,512]{1,0:T(8,128)(2,1)S(1)}, bf16[128,512]{1,0:T(8,128)(2,1)}, u32[]{:S(2)}) copy-start(bf16[128,512]{1,0:T(8,128)(2,1)} %param.14) | copy-start | bytes 393220
  14.5 28.2 %copy-start.16 = (f32[8,128]{1,0:T(8,128)S(1)}, f32[8,128]{1,0:T(8,128)}, u32[]{:S(2)}) copy-start(f32[8,128]{1,0:T(8,128)} %param.15) | copy-start | bytes 12292
  14.5 23.6 %all-to-all-start.1 = ((bf16[16,8,1,2048]{3,1,2,0:T(8,128)(2,1)}), bf16[16,8,1,2048]{3,1,2,0:T(8,128)(2,1)S(1)}, u32[]{:S(2)}, u32[]{:S(2)}) async-start(bf16[16,8,1,2048]{3,1,2,0:T(8,128)(2,1)} %get-tuple-element.28), calls=%async_computation.1 | async-start | bytes 1048576 | tf_op jit(solution)/shard_map/all_to_all | solution.py:78
  23.0 20.8 %copy-start.15 = (bf16[128,512]{1,0:T(8,128)(2,1)S(1)}, bf16[128,512]{1,0:T(8,128)(2,1)}, u32[]{:S(2)}) copy-start(bf16[128,512]{1,0:T(8,128)(2,1)} %param.11) | copy-start | bytes 393220
  23.2 22.0 %copy-start.12 = (bf16[128,1024]{1,0:T(8,128)(2,1)S(1)}, bf16[128,1024]{1,0:T(8,128)(2,1)}, u32[]{:S(2)}) copy-start(bf16[128,1024]{1,0:T(8,128)(2,1)} %param.17) | copy-start | bytes 786436
  38.0 18.4 %all-to-all-start = ((bf16[16,8,1,2048]{3,1,2,0:T(8,128)(2,1)}), bf16[16,8,1,2048]{3,1,2,0:T(8,128)(2,1)S(1)}, u32[]{:S(2)}, u32[]{:S(2)}) async-start(bf16[16,8,1,2048]{3,1,2,0:T(8,128)(2,1)} %get-tuple-element.29), calls=%async_computation | async-start | bytes 1048576 | tf_op jit(solution)/shard_map/all_to_all | solution.py:77
  42.0 161.6 %reduce-scatter.2.cloned.1.call-start = ((), (), s32[]{:S(2)}) async-start(), calls=%async_computation.5 | async-start | bytes 4456448 | tf_op jit(solution)/shard_map/reduce_scatter | solution.py:162
  77.1 2.3 %copy-start.5 = (bf16[8,4,384,64]{2,3,1,0:T(8,128)(2,1)S(1)}, bf16[8,4,384,64]{2,3,1,0:T(8,128)(2,1)}, u32[]{:S(2)}) copy-start(bf16[8,4,384,64]{2,3,1,0:T(8,128)(2,1)} %copy.89) | copy-start | bytes 4718596
  77.1 2.3 %copy-start.6 = (bf16[4,32,8,64]{3,2,1,0:T(8,128)(2,1)S(1)}, bf16[4,32,8,64]{3,2,1,0:T(8,128)(2,1)}, u32[]{:S(2)}) copy-start(bf16[4,32,8,64]{3,2,1,0:T(8,128)(2,1)} %reshape.196) | copy-start | bytes 393220
  77.1 2.3 %copy-start.11 = (bf16[4,32,8,64]{1,3,0,2:T(8,128)(2,1)S(1)}, bf16[4,32,8,64]{1,3,0,2:T(8,128)(2,1)}, u32[]{:S(2)}) copy-start(bf16[4,32,8,64]{1,3,0,2:T(8,128)(2,1)} %copy.88) | copy-start | bytes 393220
  80.6 1.3 copy-start.2
  81.9 1.1 copy-start.4
  83.0 2.8 %copy-start.10 = (bf16[128,512]{1,0:T(8,128)(2,1)}, bf16[128,512]{1,0:T(8,128)(2,1)S(1)}, u32[]{:S(2)}) copy-start(bf16[128,512]{1,0:T(8,128)(2,1)S(1)} %convert_element_type.43) | copy-start | bytes 393220
  85.8 1.0 copy-start.7
  87.5 2.1 copy-start.1
  100.6 12.3 %copy-start.3 = (f32[8,4,32,416]{3,2,1,0:T(8,128)S(1)}, f32[8,4,32,416]{3,2,1,0:T(8,128)}, u32[]{:S(2)}) copy-start(f32[8,4,32,416]{3,2,1,0:T(8,128)} %copy-done.2) | copy-start | bytes 5111812
  108.5 34.6 %all-to-all-start.2 = ((f32[16,8,1,2048]{3,1,2,0:T(8,128)}), f32[16,8,1,2048]{3,1,2,0:T(8,128)}, u32[]{:S(2)}, u32[]{:S(2)}) async-start(f32[16,8,1,2048]{3,1,2,0:T(8,128)} %bitcast.23), calls=%async_computation.2 | async-start | bytes 2097152 | tf_op jit(solution)/shard_map/all_to_all | solution.py:143
  113.7 2.0 copy-start
  143.1 40.8 %all-to-all-start.3 = ((f32[16,8,1,2048]{3,1,2,0:T(8,128)}), f32[16,8,1,2048]{3,1,2,0:T(8,128)S(1)}, u32[]{:S(2)}, u32[]{:S(2)}) async-start(f32[16,8,1,2048]{3,1,2,0:T(8,128)} %bitcast.31), calls=%async_computation.3 | async-start | bytes 2097152 | tf_op jit(solution)/shard_map/all_to_all | solution.py:144
Sparse Core Ops, SparseCore 0:
  85.9 117.6 reduce-scatter.1
where the time goes:
time: 213 us; the launch traced here: 212 us
  waiting for transfers between devices  70.6 us (33%)
  local copies, waits for them, and re-layouts  63.6 us (30%)
  starting transfers between devices  27.2 us (13%)
  other arithmetic  22.5 us (11%)
  between operations  14.6 us (7%)
  matrix products  11.4 us (5%)
  blocking collectives  2.49 us (1%)
    all_to_all x1, waiting for transfers between devices, body(): lax.all_to_all(to_slots(value_grad), 'kv', split_axis=0, concat_axis=0, t...  24.2 us
    reduce_scatter x1, waiting for transfers between devices, body(): lax.psum_scatter(lax.dot_general(whole_input, grad_queries, (((0,), (0,))...  14.9 us
    scatter-add x2, other arithmetic, to_slots(): jax.ops.segment_sum(chosen_part, tile_ids, num_segments=devices * head_co...  14.2 us
    all_to_all x1, waiting for transfers between devices, body(): lax.all_to_all(value_send, 'kv', split_axis=0, concat_axis=0, tiled=True)  13.6 us
    all_to_all x1, waiting for transfers between devices, body(): lax.all_to_all(to_slots(key_grad), 'kv', split_axis=0, concat_axis=0, til...  11.6 us
    reshape x2, local copies, waits for them, and re-layouts, to_slots(): chosen_part = gradient[:, :, :SEL * BLK].reshape(-1, tile_size)  11.4 us
    all_to_all x1, starting transfers between devices, body(): lax.all_to_all(to_slots(value_grad), 'kv', split_axis=0, concat_axis=0, t...  10.4 us
    slice x4, local copies, waits for them, and re-layouts, to_slots(): chosen_part = gradient[:, :, :SEL * BLK].reshape(-1, tile_size)  9.19 us
  transfers between devices with their start and end apart: 5, of which 5 were waited for; matrix products, arithmetic and copies ran while one was open for 26% of the time, Pallas kernels for 0%

commit v1 on v0

v1 whole, which is shorter than its diff:
```python
import functools

import jax
import jax.numpy as jnp
from jax import lax
from jax.experimental import pallas as pl
from jax.experimental.pallas import tpu as pltpu
from jax.sharding import PartitionSpec as P

HD = 64
BLK = 32
MASKED = -1e30
MESH = pl.DeviceIdType.MESH
F32 = jnp.float32
BF16 = jnp.bfloat16


def dot(a, b, ca, cb):
    return lax.dot_general(a, b, (((ca,), (cb,)), ((), ())), preferred_element_type=F32)


def kernel(
    n, tp, g, q_ref, k_ref, v_ref, c_ref, bias_ref, hot_ref, x_ref,
    gq_ref, gk_ref, gv_ref, gw_ref,
    ks, vs, kt, vt, dvs, dks, dvr, dkr, wt, wo, gko, gvo, qs, cs, xs, xr, dqr, gs, gr,
    ssem, rsem, xssem, xrsem, gssem, grsem,
):
    r = n // g
    tok, cols = q_ref.shape
    bd = tok // BLK
    pairs = cols // (2 * HD)
    wide = 2 * HD
    scale = HD ** (-0.5)
    rt = r // tp
    w = x_ref.shape[1] // (rt * g)
    me, t = lax.axis_index("kv"), lax.axis_index("tp")
    z, j = me // g, lax.rem(me, g)

    def tile_copy(kind, src, dst, there, slot):
        return pltpu.make_async_remote_copy(
            src_ref=src, dst_ref=dst, send_sem=ssem.at[kind, there], recv_sem=rsem.at[kind, slot],
            device_id=(there, t), device_id_type=MESH)

    def picked(ref, d):
        out = None
        for b in range(bd):
            hot = jnp.broadcast_to(hot_ref[d, b : b + 1, :], (BLK, cols)).astype(BF16)
            term = ref[b * BLK : (b + 1) * BLK, :] * hot
            out = term if out is None else out + term
        return out

    def send_all(kind, ref, buf, landing):
        def step(i, carry):
            d = n - 1 - i
            buf[d] = picked(ref, d)
            tile_copy(kind, buf.at[d], landing.at[me], d, me).start()
            return carry
        lax.fori_loop(0, n - 1 - me, step, 0)

    def each_lower(fn):
        def step(o, carry):
            fn(o)
            return carry
        lax.fori_loop(0, me, step, 0)

    def each_upper(fn):
        def step(d, carry):
            fn(d)
            return carry
        lax.fori_loop(me + 1, n, step, 0)

    send_all(0, k_ref, ks, kt)
    send_all(1, v_ref, vs, vt)

    def clear(o, carry):
        kt[o] = jnp.zeros(kt.shape[1:], BF16)
        vt[o] = jnp.zeros(vt.shape[1:], BF16)
        return carry
    lax.fori_loop(me, n, clear, 0)

    for p in range(g):
        for zl in range(rt):
            at = (zl * g + p) * w
            xs[p, zl] = x_ref[:, at : at + w]

    def x_copy(p, t2):
        return pltpu.make_async_remote_copy(
            src_ref=xs.at[p], dst_ref=xr.at[j, pl.ds(t * rt, rt)],
            send_sem=xssem.at[p, t2], recv_sem=xrsem.at[j, t],
            device_id=(z * g + p, t2), device_id_type=MESH)

    def x_landed(p, t2):
        return pltpu.make_async_remote_copy(
            src_ref=xs.at[p], dst_ref=xr.at[p, pl.ds(t2 * rt, rt)],
            send_sem=xssem.at[p, t2], recv_sem=xrsem.at[p, t2],
            device_id=(z * g + p, t2), device_id_type=MESH)

    def each_x(fn):
        def step(i, carry):
            p, t2 = i // tp, lax.rem(i, tp)

            @pl.when((p != j) | (t2 != t))
            def _():
                fn(p, t2)
            return carry
        lax.fori_loop(0, g * tp, step, 0)

    each_x(lambda p, t2: x_copy(p, t2).start())
    xr[j, pl.ds(t * rt, rt)] = xs[j]

    low = lax.broadcasted_iota(jnp.int32, (tok, wide), 1) < HD
    for h in range(pairs):
        c = h * wide
        qp, cp = q_ref[:, c : c + wide], c_ref[:, c : c + wide]
        zero = jnp.zeros_like(qp)
        qs[h, :tok], qs[h, tok:] = jnp.where(low, qp, zero), jnp.where(low, zero, qp)
        cs[h, :tok], cs[h, tok:] = jnp.where(low, cp, zero), jnp.where(low, zero, cp)

    key_at = lax.broadcasted_iota(jnp.int32, (tok, 2 * tok), 0)
    query_at = lax.rem(lax.broadcasted_iota(jnp.int32, (tok, 2 * tok), 1), tok)
    causal = (key_at // BLK == query_at // BLK) & (key_at <= query_at)
    rows = n * BLK

    for h in range(pairs):
        c = h * wide
        so = dot(k_ref[:, c : c + wide], qs[h], 1, 1) * scale
        ob = jnp.broadcast_to(bias_ref[h, n : n + bd], (bd, BLK, 2 * tok)).reshape(tok, 2 * tok)
        ob = jnp.where(causal, bias_ref[h, n + bd], ob)
        weights = jnp.exp(so + ob)
        wo[h] = weights
        gvo[:, c : c + wide] = dot(weights.astype(BF16), cs[h], 1, 0)

    each_lower(lambda o: tile_copy(0, ks.at[o], kt.at[o], o, o).wait_recv())
    for h in range(pairs):
        c = h * wide
        kp = kt[:, :, c : c + wide].reshape(rows, wide)
        st = (dot(kp, qs[h], 1, 1) * scale).reshape(n, BLK, 2 * tok)
        weights = jnp.exp(st + bias_ref[h, :n]).reshape(rows, 2 * tok)
        wt[h] = weights
        dvs[:, :, c : c + wide] = dot(weights.astype(BF16), cs[h], 1, 0).astype(BF16).reshape(n, BLK, wide)
    each_lower(lambda o: tile_copy(2, dvs.at[o], dvr.at[me], o, me).start())

    each_lower(lambda o: tile_copy(1, vs.at[o], vt.at[o], o, o).wait_recv())
    for h in range(pairs):
        c = h * wide
        vp = vt[:, :, c : c + wide].reshape(rows, wide)
        kp = kt[:, :, c : c + wide].reshape(rows, wide)
        vdt = dot(vp, cs[h], 1, 1)
        vdo = dot(v_ref[:, c : c + wide], cs[h], 1, 1)
        weights, own = wt[h], wo[h]
        delta = jnp.sum(weights * vdt, axis=0, keepdims=True) + jnp.sum(own * vdo, axis=0, keepdims=True)
        dst = (weights * (vdt - delta)).astype(BF16)
        dso = (own * (vdo - delta)).astype(BF16)
        dq = (dot(dst, kp, 0, 0) + dot(dso, k_ref[:, c : c + wide], 0, 0)) * scale
        dq = jnp.where(low, dq[:tok], dq[tok:]).astype(BF16)
        gq_ref[:, c : c + wide] = dq
        dqr[j, :, c : c + wide] = dq
        dks[:, :, c : c + wide] = (dot(dst, qs[h], 1, 0) * scale).astype(BF16).reshape(n, BLK, wide)
        gko[:, c : c + wide] = dot(dso, qs[h], 1, 0) * scale

    def dq_copy(p, slot):
        return pltpu.make_async_remote_copy(
            src_ref=dqr.at[j], dst_ref=dqr.at[slot], send_sem=gssem.at[0, p], recv_sem=grsem.at[0, slot],
            device_id=(z * g + p, t), device_id_type=MESH)

    for i in range(1, g):
        dq_copy(lax.rem(j + i, g), j).start()
    each_lower(lambda o: tile_copy(3, dks.at[o], dkr.at[me], o, me).start())

    each_x(lambda p, t2: x_landed(p, t2).wait_recv())
    for i in range(1, g):
        p = lax.rem(j + i, g)
        dq_copy(p, p).wait_recv()

    def partial(zz):
        return dot(xr[:, zz].reshape(g * tok, w), dqr[...].reshape(g * tok, cols), 0, 0)

    def gw_copy(zz, slot):
        return pltpu.make_async_remote_copy(
            src_ref=gs.at[zz], dst_ref=gr.at[slot], send_sem=gssem.at[1, zz], recv_sem=grsem.at[1, slot],
            device_id=(zz * g + j, t), device_id_type=MESH)

    for i in range(1, r):
        zz = lax.rem(z + i, r)
        gs[zz] = partial(zz).astype(BF16)
        gw_copy(zz, z).start()
    gw_ref[...] = partial(z)

    def settle(kind, held, landed, own, out):
        def add(d):
            tile_copy(kind, held.at[d], landed.at[d], d, d).wait_recv()
            tile = landed[d].astype(F32)
            for b in range(bd):
                own[b * BLK : (b + 1) * BLK, :] += tile * hot_ref[d, b : b + 1, :]
        each_upper(add)
        out[...] = own[...].astype(BF16)

    settle(2, dvs, dvr, gvo, gv_ref)
    settle(3, dks, dkr, gko, gk_ref)
    for i in range(1, r):
        zz = lax.rem(z + i, r)
        gw_copy(zz, zz).wait_recv()
        gw_ref[...] += gr[zz].astype(F32)

    each_upper(lambda d: tile_copy(0, ks.at[d], kt.at[me], d, me).wait_send())
    each_upper(lambda d: tile_copy(1, vs.at[d], vt.at[me], d, me).wait_send())
    each_lower(lambda o: tile_copy(2, dvs.at[o], dvr.at[me], o, me).wait_send())
    each_lower(lambda o: tile_copy(3, dks.at[o], dkr.at[me], o, me).wait_send())
    each_x(lambda p, t2: x_copy(p, t2).wait_send())
    for i in range(1, g):
        dq_copy(lax.rem(j + i, g), j).wait_send()
    for i in range(1, r):
        gw_copy(lax.rem(z + i, r), z).wait_send()


def body(n, tp, g, queries, keys, values, cotangent, log_sum, chosen, normed_input):
    tok, cols = queries.shape
    heads = log_sum.shape[0]
    bd = tok // BLK
    pairs = heads // 2
    r = n // g
    sel = chosen.shape[2]
    me = lax.axis_index("kv")
    blocks = chosen.shape[1]
    ids = jnp.arange(blocks, dtype=jnp.int32)
    devs = jnp.arange(n, dtype=jnp.int32)
    own_ids = me * bd + jnp.arange(bd, dtype=jnp.int32)
    mine = lax.dynamic_slice_in_dim(chosen, me * bd, bd, 1)
    usable = mine < own_ids[None, :, None]
    owner = jnp.where(usable, mine // bd, n)
    tile_need = jnp.any(owner[:, None] == devs[None, :, None, None], axis=3) & (devs < me)[None, :, None]
    own_need = jnp.any((mine[:, None] == own_ids[None, :, None, None]) & usable[:, None], axis=3)
    need = jnp.concatenate([tile_need, own_need, jnp.ones((heads, 1, bd), bool)], axis=1)
    less = -log_sum.reshape(heads, 1, bd, BLK)
    bias = jnp.where(need[..., None], less, MASKED).reshape(pairs, 2, n + bd + 1, tok)
    bias = bias.transpose(0, 2, 1, 3).reshape(pairs, n + bd + 1, 1, 2 * tok)
    grouped = chosen.reshape(heads, n, 1, bd * sel)
    hot = jnp.any(grouped == own_ids[None, None, :, None], axis=3) & (devs > me)[None, :, None]
    hot = jnp.repeat(hot.transpose(1, 2, 0).astype(F32), HD, axis=2)
    w = normed_input.shape[1] // (r // tp * g)
    tile = (n, BLK, cols)
    vmem = pl.BlockSpec(memory_space=pltpu.VMEM)
    return pl.pallas_call(
        functools.partial(kernel, n, tp, g),
        out_shape=[
            jax.ShapeDtypeStruct((tok, cols), BF16),
            jax.ShapeDtypeStruct((tok, cols), BF16),
            jax.ShapeDtypeStruct((tok, cols), BF16),
            jax.ShapeDtypeStruct((w, cols), F32),
        ],
        in_specs=[vmem] * 7,
        out_specs=[vmem] * 4,
        scratch_shapes=[pltpu.VMEM(tile, BF16)] * 8
        + [
            pltpu.VMEM((pairs, n * BLK, 2 * tok), F32),
            pltpu.VMEM((pairs, tok, 2 * tok), F32),
            pltpu.VMEM((tok, cols), F32),
            pltpu.VMEM((tok, cols), F32),
            pltpu.VMEM((pairs, 2 * tok, 2 * HD), BF16),
            pltpu.VMEM((pairs, 2 * tok, 2 * HD), BF16),
            pltpu.VMEM((g, r // tp, tok, w), BF16),
            pltpu.VMEM((g, r, tok, w), BF16),
            pltpu.VMEM((g, tok, cols), BF16),
            pltpu.VMEM((r, w, cols), BF16),
            pltpu.VMEM((r, w, cols), BF16),
            pltpu.SemaphoreType.DMA((4, n)),
            pltpu.SemaphoreType.DMA((4, n)),
            pltpu.SemaphoreType.DMA((g, tp)),
            pltpu.SemaphoreType.DMA((g, tp)),
            pltpu.SemaphoreType.DMA((2, max(g, r))),
            pltpu.SemaphoreType.DMA((2, max(g, r))),
        ],
        compiler_params=pltpu.CompilerParams(has_side_effects=True, vmem_limit_bytes=48 * 1024 * 1024),
    )(queries, keys, values, cotangent, bias, hot, normed_input)


def solution(mesh):
    n, tp = mesh.shape["kv"], mesh.shape["tp"]
    g = 1
    while 4 * g * g <= n:
        g *= 2
    in_specs = (
        P("kv", "tp"), P("kv", "tp"), P("kv", "tp"), P("kv", "tp"),
        P("tp", "kv"), P("tp", None, None), P("kv", "tp"),
    )
    out_specs = (P("kv", "tp"),) * 4
    return jax.shard_map(
        functools.partial(body, n, tp, g), mesh=mesh, in_specs=in_specs, out_specs=out_specs, check_vma=False
    )
```

time: 213 us -> 71.5 us (0.34)
  waiting for transfers between devices: 70.6 us -> 0 us
  Pallas kernels: 0 us -> 61.3 us
  local copies, waits for them, and re-layouts: 63.6 us -> 6.75 us
  starting transfers between devices: 27.2 us -> 0 us
  other arithmetic: 22.5 us -> 2.3 us
  between operations: 14.6 us -> 0.8 us
  matrix products: 11.4 us -> 0 us
  blocking collectives: 2.49 us -> 0 us
    pallas_call x0 -> x1, Pallas kernels: none -> 61.3 us  [body(): pl.pallas_call(functools.partial(kernel, n, tp, g), out_shape=[jax.ShapeD...]
    all_to_all x4 -> x0, waiting for transfers between devices: 55.6 us -> none  [the longest x1 24.2 us: body(): lax.all_to_all(to_slots(value_grad), 'kv', split_axis=0, concat_axis=0, t...]
    reshape x20 -> x1, local copies, waits for them, and re-layouts: 31.2 us -> 0.13 us  [body(): hot = jnp.repeat(hot.transpose(1, 2, 0).astype(F32), HD, axis=2)]
    all_to_all x4 -> x0, starting transfers between devices: 27.2 us -> none  [the longest x1 10.4 us: body(): lax.all_to_all(to_slots(value_grad), 'kv', split_axis=0, concat_axis=0, t...]
    reduce_scatter x1 -> x0, waiting for transfers between devices: 14.9 us -> none  [body(): lax.psum_scatter(lax.dot_general(whole_input, grad_queries, (((0,), (0,))...]
    scatter-add x2 -> x0, other arithmetic: 14.2 us -> none  [to_slots(): jax.ops.segment_sum(chosen_part, tile_ids, num_segments=devices * head_co...]
    dot_general x8 -> x0, matrix products: 11.4 us -> none  [the longest x2 3.13 us: settle(): jnp.dot(targets, flat_tiles, precision=lax.Precision.HIGHEST, preferred_e...]
    slice x4 -> x0, local copies, waits for them, and re-layouts: 9.19 us -> none  [to_slots(): chosen_part = gradient[:, :, :SEL * BLK].reshape(-1, tile_size)]
  transfers between devices with their start and end apart: 5 -> 0, of which waited for: 5 -> 0; matrix products, arithmetic and copies ran while one was open for 26% -> 0% of each run, Pallas kernels for 0% -> 0%
where the time goes in v1:
time: 71.5 us; the launch traced here: 71.2 us
  Pallas kernels  61.3 us (86%)
  local copies, waits for them, and re-layouts  6.75 us (9%)
  other arithmetic  2.3 us (3%)
  between operations  0.8 us (1%)
    pallas_call x1, Pallas kernels, body(): pl.pallas_call(functools.partial(kernel, n, tp, g), out_shape=[jax.ShapeD...  61.3 us
    unnamed x19, local copies, waits for them, and re-layouts  5.02 us

profile of v1, /device:TPU:0, one launch (start us, length us, event | category | flops | bytes accessed | tf_op | source)
XLA Modules:
  0.0 71.2 jit_solution(5334926247767231213)
XLA Ops:
  0.6 0.0 copy-start.6
  0.7 0.1 pad.2.clone
  0.7 0.6 copy-done.6
  1.3 0.9 %fusion.2 = (s32[8,4,12]{1,0,2:T(8,128)S(1)}, s32[8,4,12]{1,0,2:T(8,128)S(1)}) fusion(s32[4]{0:T(128)S(1)} %iota_add_fusion, s32[8,64,12]{1,0,2:T(8,128)} %param.12, s32[]{:T(128)S(6)} %select_n.17), kind=kLoop, calls=%fused_computation.10 | loop fusion | flops 6528 | bytes 4628 | tf_op jit(solution)/shard_map/jit(_where)/select_n | solution.py:230
  2.2 0.2 copy.33
  2.4 0.1 fusion
  2.6 0.1 copy.34
  2.7 0.1 copy.35
  2.9 0.4 and_reduce_fusion
  3.3 0.1 copy.36
  3.4 0.1 add_add_fusion
  3.5 0.2 copy.37
  3.7 0.2 broadcast_in_dim.44
  3.9 0.2 broadcast_in_dim.45
  4.1 0.0 copy-start.5
  4.2 0.7 %copy-done.5 = s32[8,64,12]{1,0,2:T(8,128)S(1)} copy-done((s32[8,64,12]{1,0,2:T(8,128)S(1)}, s32[8,64,12]{1,0,2:T(8,128)}, u32[]{:S(2)}) %copy-start.5) | copy-done | bytes 24600
  4.9 0.1 copy.39
  5.1 0.1 eq.47
  5.2 0.0 copy-start.4
  5.2 0.7 compare_reduce_fusion
  5.9 0.1 copy.40
  6.0 0.0 copy-start.2
  6.0 0.0 copy-start.3
  6.0 0.1 broadcast_in_dim.48
  6.2 0.0 copy-start
  6.2 0.0 copy-start.1
  6.2 0.1 reshape.54.hot_ref
  6.3 0.0 copy-done.4
  6.3 0.6 copy-done.2
  6.9 0.1 copy-done.3
  7.0 0.1 copy-done
  7.1 0.0 copy-done.1
  7.2 61.3 %shard_map.102 = (bf16[128,512]{1,0:T(8,128)(2,1)S(1)}, bf16[128,512]{1,0:T(8,128)(2,1)S(1)}, bf16[128,512]{1,0:T(8,128)(2,1)S(1)}, f32[128,512]{1,0:T(8,128)S(1)}) custom-call(bf16[128,512]{1,0:T(8,128)(2,1)S(1)} %copy-done.1, bf16[128,512]{1,0:T(8,128)(2,1)S(1)} %copy-done.2, bf16[128,512]{1,0:T(8,128)(2,1)S(1)} %copy-done.3, ...), custom_call_target="tpu_custom_call" | custom-call | tf_op jit(solution)/shard_map/pallas_call | solution.py:243
  68.5 0.7 copy.45
  69.2 0.7 copy.46
  69.8 0.7 copy.47
  70.5 0.7 copy.48
  (8 shorter events, 0.1 us)
Async XLA Ops:
  0.6 0.7 copy-start.6
  4.1 0.8 %copy-start.5 = (s32[8,64,12]{1,0,2:T(8,128)S(1)}, s32[8,64,12]{1,0,2:T(8,128)}, u32[]{:S(2)}) copy-start(s32[8,64,12]{1,0,2:T(8,128)} %param.12) | copy-start | bytes 73732
  5.2 1.1 %copy-start.4 = (bf16[128,512]{1,0:T(8,128)(2,1)S(1)}, bf16[128,512]{1,0:T(8,128)(2,1)}, u32[]{:S(2)}) copy-start(bf16[128,512]{1,0:T(8,128)(2,1)} %c_ref.1) | copy-start | bytes 393220
  6.0 0.9 %copy-start.2 = (bf16[128,512]{1,0:T(8,128)(2,1)S(1)}, bf16[128,512]{1,0:T(8,128)(2,1)}, u32[]{:S(2)}) copy-start(bf16[128,512]{1,0:T(8,128)(2,1)} %k_ref.1) | copy-start | bytes 393220
  6.0 1.0 %copy-start.3 = (bf16[128,512]{1,0:T(8,128)(2,1)S(1)}, bf16[128,512]{1,0:T(8,128)(2,1)}, u32[]{:S(2)}) copy-start(bf16[128,512]{1,0:T(8,128)(2,1)} %v_ref.1) | copy-start | bytes 393220
  6.2 1.0 %copy-start = (bf16[128,1024]{1,0:T(8,128)(2,1)S(1)}, bf16[128,1024]{1,0:T(8,128)(2,1)}, u32[]{:S(2)}) copy-start(bf16[128,1024]{1,0:T(8,128)(2,1)} %x_ref.1) | copy-start | bytes 786436
  6.2 1.0 %copy-start.1 = (bf16[128,512]{1,0:T(8,128)(2,1)S(1)}, bf16[128,512]{1,0:T(8,128)(2,1)}, u32[]{:S(2)}) copy-start(bf16[128,512]{1,0:T(8,128)(2,1)} %q_ref.1) | copy-start | bytes 393220

commit v2 on v1

v2 whole, which is shorter than its diff:
```python
import functools

import jax
import jax.numpy as jnp
from jax import lax
from jax.experimental import pallas as pl
from jax.experimental.pallas import tpu as pltpu
from jax.sharding import PartitionSpec as P

HD = 64
BLK = 32
MASKED = -1e30
MESH = pl.DeviceIdType.MESH
F32 = jnp.float32
BF16 = jnp.bfloat16


def dot(a, b, ca, cb):
    return lax.dot_general(a, b, (((ca,), (cb,)), ((), ())), preferred_element_type=F32)


def kernel(
    n, tp, g, q_ref, k_ref, v_ref, c_ref, lse_ref, pick_ref, x_ref,
    gq_ref, gk_ref, gv_ref, gw_ref,
    bias, hot, kvs, kvt, dkvs, dkvr, gko, gvo, xs, xr, dqr, gs, gr,
    ssem, rsem, xssem, xrsem, dssem, drsem, gssem, grsem,
):
    r = n // g
    tok, cols = q_ref.shape
    sel, heads, blocks = pick_ref.shape
    bd = tok // BLK
    wide = 2 * HD
    pairs = cols // wide
    scale = HD ** (-0.5)
    rt = r // tp
    w = x_ref.shape[1] // (rt * g)
    me, t = lax.axis_index("kv"), lax.axis_index("tp")
    z, j = me // g, lax.rem(me, g)
    rows = n * BLK

    def iota(shape, dim):
        return lax.broadcasted_iota(jnp.int32, shape, dim)

    def each(low, high, fn):
        def step(i, carry):
            fn(i)
            return carry
        lax.fori_loop(low, high, step, 0)

    def kv_copy(h, there, slot):
        return pltpu.make_async_remote_copy(
            src_ref=kvs.at[h, there], dst_ref=kvt.at[h, slot], send_sem=ssem.at[0, h, there],
            recv_sem=rsem.at[0, h, slot], device_id=(there, t), device_id_type=MESH)

    def back_copy(h, there, slot):
        return pltpu.make_async_remote_copy(
            src_ref=dkvs.at[h, there], dst_ref=dkvr.at[h, slot], send_sem=ssem.at[1, h, there],
            recv_sem=rsem.at[1, h, slot], device_id=(there, t), device_id_type=MESH)

    def x_copy(p, t2, at, t3):
        return pltpu.make_async_remote_copy(
            src_ref=xs.at[p], dst_ref=xr.at[at, pl.ds(t3 * rt, rt)],
            send_sem=xssem.at[p, t2], recv_sem=xrsem.at[at, t3],
            device_id=(z * g + p, t2), device_id_type=MESH)

    def dq_copy(h, p, slot):
        return pltpu.make_async_remote_copy(
            src_ref=dqr.at[h, j], dst_ref=dqr.at[h, slot], send_sem=dssem.at[h, p], recv_sem=drsem.at[h, slot],
            device_id=(z * g + p, t), device_id_type=MESH)

    def gw_copy(h, zz, slot):
        return pltpu.make_async_remote_copy(
            src_ref=gs.at[h, zz], dst_ref=gr.at[h, slot], send_sem=gssem.at[h, zz], recv_sem=grsem.at[h, slot],
            device_id=(zz * g + j, t), device_id_type=MESH)

    def each_x(fn):
        def step(i):
            p, t2 = i // tp, lax.rem(i, tp)

            @pl.when((p != j) | (t2 != t))
            def _():
                fn(p, t2)
        each(0, g * tp, step)

    pool = (iota((blocks, n), 0) // bd == iota((blocks, n), 1)).astype(BF16)
    spread = (iota((heads, cols), 1) // HD == iota((heads, cols), 0)).astype(BF16)
    later = iota((n, cols), 0) > me
    for b in range(bd):
        hit = jnp.zeros((heads, blocks), jnp.bool_)
        for s in range(sel):
            hit = hit | (pick_ref[s] == me * bd + b)
        count = dot(jnp.where(hit, 1.0, 0.0).astype(BF16), pool, 1, 0)
        taken = dot(count.astype(BF16), spread, 0, 0)
        hot[:, b, :] = jnp.where((taken > 0.5) & later, 1.0, 0.0)

    def picked(ref, d, c):
        out = None
        for b in range(bd):
            one = jnp.broadcast_to(hot[d, b : b + 1, c : c + wide], (BLK, wide)).astype(BF16)
            term = ref[b * BLK : (b + 1) * BLK, c : c + wide] * one
            out = term if out is None else out + term
        return out

    def send_kv(h):
        def step(i):
            d = n - 1 - i
            kvs[h, d, 0] = picked(k_ref, d, h * wide)
            kvs[h, d, 1] = picked(v_ref, d, h * wide)
            kv_copy(h, d, me).start()
        each(0, n - 1 - me, step)

    for h in range(pairs):
        send_kv(h)

    for p in range(g):
        for zl in range(rt):
            at = (zl * g + p) * w
            xs[p, zl] = x_ref[:, at : at + w]
    each_x(lambda p, t2: x_copy(p, t2, j, t).start())
    xr[j, pl.ds(t * rt, rt)] = xs[j]

    def clear(o):
        for h in range(pairs):
            kvt[h, o] = jnp.zeros(kvt.shape[2:], BF16)
    each(me, n, clear)

    at_block = me * bd + iota((blocks, tok), 1) // BLK
    mine = (iota((blocks, tok), 0) == at_block).astype(F32)
    ids = pick_ref[...].astype(F32).reshape(sel * heads, blocks)
    ids = dot(ids.astype(BF16), mine.astype(BF16), 1, 0)
    ids = (ids + 0.5).astype(jnp.int32).reshape(sel, heads, tok)
    ids = jnp.where(ids < me * bd + iota(ids.shape, 2) // BLK, ids, n * bd)
    owner = ids // bd
    less = -lse_ref[...]

    def put(row, need):
        line = less if need is None else jnp.where(need, less, MASKED)
        for h in range(heads):
            bias[h // 2, row, :, (h % 2) * tok : (h % 2 + 1) * tok] = line[h : h + 1, :]

    for o in range(n):
        need = jnp.zeros((heads, tok), jnp.bool_)
        for s in range(sel):
            need = need | (owner[s] == o)
        put(o, need & (jnp.zeros((heads, tok), jnp.int32) + o < me))
    for b in range(bd):
        need = jnp.zeros((heads, tok), jnp.bool_)
        for s in range(sel):
            need = need | (ids[s] == me * bd + b)
        put(n + b, need)
    put(n + bd, None)

    low = iota((tok, wide), 1) < HD
    key_at = iota((tok, 2 * tok), 0)
    query_at = lax.rem(iota((tok, 2 * tok), 1), tok)
    causal = (key_at // BLK == query_at // BLK) & (key_at <= query_at)

    def stacked(ref, c):
        part = ref[:, c : c + wide]
        zero = jnp.zeros_like(part)
        return jnp.concatenate([jnp.where(low, part, zero), jnp.where(low, zero, part)], axis=0)

    def attend(h):
        c = h * wide
        qs, cs = stacked(q_ref, c), stacked(c_ref, c)
        ko, vo = k_ref[:, c : c + wide], v_ref[:, c : c + wide]
        ob = jnp.broadcast_to(bias[h, n : n + bd], (bd, BLK, 2 * tok)).reshape(tok, 2 * tok)
        ob = jnp.where(causal, bias[h, n + bd], ob)
        own = jnp.exp(dot(ko, qs, 1, 1) * scale + ob)
        vdo = dot(vo, cs, 1, 1)
        gvo[:, c : c + wide] = dot(own.astype(BF16), cs, 1, 0)
        each(0, me, lambda o: kv_copy(h, o, o).wait_recv())
        kp = kvt[h, :, 0].reshape(rows, wide)
        vp = kvt[h, :, 1].reshape(rows, wide)
        st = (dot(kp, qs, 1, 1) * scale).reshape(n, BLK, 2 * tok)
        weights = jnp.exp(st + bias[h, :n]).reshape(rows, 2 * tok)
        vdt = dot(vp, cs, 1, 1)
        dkvs[h, :, 1] = dot(weights.astype(BF16), cs, 1, 0).astype(BF16).reshape(n, BLK, wide)
        delta = jnp.sum(weights * vdt, axis=0, keepdims=True) + jnp.sum(own * vdo, axis=0, keepdims=True)
        dst = (weights * (vdt - delta)).astype(BF16)
        dso = (own * (vdo - delta)).astype(BF16)
        dq = (dot(dst, kp, 0, 0) + dot(dso, ko, 0, 0)) * scale
        dq = jnp.where(low, dq[:tok], dq[tok:]).astype(BF16)
        gq_ref[:, c : c + wide] = dq
        dqr[h, j] = dq
        dkvs[h, :, 0] = (dot(dst, qs, 1, 0) * scale).astype(BF16).reshape(n, BLK, wide)
        for i in range(1, g):
            dq_copy(h, lax.rem(j + i, g), j).start()
        each(0, me, lambda o: back_copy(h, o, me).start())
        gko[:, c : c + wide] = dot(dso, qs, 1, 0) * scale

    def weight(h):
        for i in range(1, g):
            p = lax.rem(j + i, g)
            dq_copy(h, p, p).wait_recv()
        right = dqr[h].reshape(g * tok, wide)
        for i in range(1, r):
            zz = lax.rem(z + i, r)
            gs[h, zz] = dot(xr[:, zz].reshape(g * tok, w), right, 0, 0).astype(BF16)
            gw_copy(h, zz, z).start()
        gw_ref[:, h * wide : (h + 1) * wide] = dot(xr[:, z].reshape(g * tok, w), right, 0, 0)

    for h in range(pairs):
        attend(h)
        if h == 0:
            each_x(lambda p, t2: x_copy(p, t2, p, t2).wait_recv())
        else:
            weight(h - 1)
    weight(pairs - 1)

    for h in range(pairs):
        c = h * wide

        def add(d):
            back_copy(h, d, d).wait_recv()
            dk, dv = dkvr[h, d, 0].astype(F32), dkvr[h, d, 1].astype(F32)
            for b in range(bd):
                one = hot[d, b : b + 1, c : c + wide]
                gko[b * BLK : (b + 1) * BLK, c : c + wide] += dk * one
                gvo[b * BLK : (b + 1) * BLK, c : c + wide] += dv * one
        each(me + 1, n, add)
        gk_ref[:, c : c + wide] = gko[:, c : c + wide].astype(BF16)
        gv_ref[:, c : c + wide] = gvo[:, c : c + wide].astype(BF16)
        for i in range(1, r):
            zz = lax.rem(z + i, r)
            gw_copy(h, zz, zz).wait_recv()
            gw_ref[:, c : c + wide] += gr[h, zz].astype(F32)

    for h in range(pairs):
        each(me + 1, n, lambda d: kv_copy(h, d, me).wait_send())
        each(0, me, lambda o: back_copy(h, o, me).wait_send())
        for i in range(1, g):
            dq_copy(h, lax.rem(j + i, g), j).wait_send()
        for i in range(1, r):
            gw_copy(h, lax.rem(z + i, r), z).wait_send()
    each_x(lambda p, t2: x_copy(p, t2, j, t).wait_send())


def body(n, tp, g, queries, keys, values, cotangent, log_sum, chosen, normed_input):
    tok, cols = queries.shape
    wide = 2 * HD
    pairs = cols // wide
    bd = tok // BLK
    r = n // g
    w = normed_input.shape[1] // (r // tp * g)
    tiles = pltpu.VMEM((pairs, n, 2, BLK, wide), BF16)
    vmem = pl.BlockSpec(memory_space=pltpu.VMEM)
    sem = pltpu.SemaphoreType.DMA
    return pl.pallas_call(
        functools.partial(kernel, n, tp, g),
        out_shape=[
            jax.ShapeDtypeStruct((tok, cols), BF16),
            jax.ShapeDtypeStruct((tok, cols), BF16),
            jax.ShapeDtypeStruct((tok, cols), BF16),
            jax.ShapeDtypeStruct((w, cols), F32),
        ],
        in_specs=[vmem] * 7,
        out_specs=[vmem] * 4,
        scratch_shapes=[
            pltpu.VMEM((pairs, n + bd + 1, 1, 2 * tok), F32),
            pltpu.VMEM((n, bd, cols), F32),
            tiles, tiles, tiles, tiles,
            pltpu.VMEM((tok, cols), F32),
            pltpu.VMEM((tok, cols), F32),
            pltpu.VMEM((g, r // tp, tok, w), BF16),
            pltpu.VMEM((g, r, tok, w), BF16),
            pltpu.VMEM((pairs, g, tok, wide), BF16),
            pltpu.VMEM((pairs, r, w, wide), BF16),
            pltpu.VMEM((pairs, r, w, wide), BF16),
            sem((2, pairs, n)), sem((2, pairs, n)),
            sem((g, tp)), sem((g, tp)),
            sem((pairs, g)), sem((pairs, g)),
            sem((pairs, r)), sem((pairs, r)),
        ],
        compiler_params=pltpu.CompilerParams(has_side_effects=True, vmem_limit_bytes=48 * 1024 * 1024),
    )(queries, keys, values, cotangent, log_sum, chosen.transpose(2, 0, 1), normed_input)


def solution(mesh):
    n, tp = mesh.shape["kv"], mesh.shape["tp"]
    g = 1
    while 4 * g * g <= n:
        g *= 2
    in_specs = (
        P("kv", "tp"), P("kv", "tp"), P("kv", "tp"), P("kv", "tp"),
        P("tp", "kv"), P("tp", None, None), P("kv", "tp"),
    )
    out_specs = (P("kv", "tp"),) * 4
    return jax.shard_map(
        functools.partial(body, n, tp, g), mesh=mesh, in_specs=in_specs, out_specs=out_specs, check_vma=False
    )
```

time: 71.5 us -> 70.9 us (level)
  other arithmetic: 2.3 us -> 0 us
  local copies, waits for them, and re-layouts: 6.75 us -> 8.71 us
    unnamed x19 -> x18, local copies, waits for them, and re-layouts: 5.02 us -> 8.71 us
    reduce_or x3 -> x0, other arithmetic: 1.26 us -> none  [the longest x1 0.7 us: body(): jnp.any(grouped == own_ids[None, None, :, None], axis=3)]
    select_n x1 -> x0, other arithmetic: 0.9 us -> none  [body(): owner = jnp.where(usable, mine // bd, n)]
where the time goes in v2:
time: 70.9 us; the launch traced here: 70.6 us
  Pallas kernels  61.3 us (86%)
  local copies, waits for them, and re-layouts  8.71 us (12%)
    pallas_call x1, Pallas kernels, body(): pl.pallas_call(functools.partial(kernel, n, tp, g), out_shape=[jax.ShapeD...  61.3 us
    unnamed x18, local copies, waits for them, and re-layouts  8.71 us

profile of v2, /device:TPU:0, one launch (start us, length us, event | category | flops | bytes accessed | tf_op | source)
XLA Modules:
  0.0 70.6 jit_solution(5267730752544750474)
XLA Ops:
  0.6 0.0 copy-start
  0.6 0.9 %copy-done = bf16[128,1024]{1,0:T(8,128)(2,1)S(1)} copy-done((bf16[128,1024]{1,0:T(8,128)(2,1)S(1)}, bf16[128,1024]{1,0:T(8,128)(2,1)}, u32[]{:S(2)}) %copy-start) | copy-done | bytes 262168
  1.6 0.0 copy-start.1
  1.6 0.9 %copy-done.1 = bf16[128,512]{1,0:T(8,128)(2,1)S(1)} copy-done((bf16[128,512]{1,0:T(8,128)(2,1)S(1)}, bf16[128,512]{1,0:T(8,128)(2,1)}, u32[]{:S(2)}) %copy-start.1) | copy-done | bytes 131096
  2.5 0.0 copy-start.2
  2.5 0.9 %copy-done.2 = bf16[128,512]{1,0:T(8,128)(2,1)S(1)} copy-done((bf16[128,512]{1,0:T(8,128)(2,1)S(1)}, bf16[128,512]{1,0:T(8,128)(2,1)}, u32[]{:S(2)}) %copy-start.2) | copy-done | bytes 131096
  3.4 0.0 copy-start.3
  3.4 0.9 %copy-done.3 = bf16[128,512]{1,0:T(8,128)(2,1)S(1)} copy-done((bf16[128,512]{1,0:T(8,128)(2,1)S(1)}, bf16[128,512]{1,0:T(8,128)(2,1)}, u32[]{:S(2)}) %copy-start.3) | copy-done | bytes 131096
  4.3 0.0 copy-start.4
  4.3 0.9 %copy-done.4 = bf16[128,512]{1,0:T(8,128)(2,1)S(1)} copy-done((bf16[128,512]{1,0:T(8,128)(2,1)S(1)}, bf16[128,512]{1,0:T(8,128)(2,1)}, u32[]{:S(2)}) %copy-start.4) | copy-done | bytes 131096
  5.2 0.0 copy-start.5
  5.2 0.8 %copy-done.5 = s32[8,64,12]{1,0,2:T(8,128)S(1)} copy-done((s32[8,64,12]{1,0,2:T(8,128)S(1)}, s32[8,64,12]{1,0,2:T(8,128)}, u32[]{:S(2)}) %copy-start.5) | copy-done | bytes 24600
  6.0 0.0 copy-start.6
  6.0 0.7 copy-done.6
  6.7 61.3 %shard_map.102 = (bf16[128,512]{1,0:T(8,128)(2,1)S(1)}, bf16[128,512]{1,0:T(8,128)(2,1)S(1)}, bf16[128,512]{1,0:T(8,128)(2,1)S(1)}, f32[128,512]{1,0:T(8,128)S(1)}) custom-call(bf16[128,512]{1,0:T(8,128)(2,1)S(1)} %copy-done.1, bf16[128,512]{1,0:T(8,128)(2,1)S(1)} %copy-done.2, bf16[128,512]{1,0:T(8,128)(2,1)S(1)} %copy-done.3, ...), custom_call_target="tpu_custom_call" | custom-call | tf_op jit(solution)/shard_map/pallas_call | solution.py:249
  68.0 0.7 copy.15
  68.6 0.7 copy.16
  69.3 0.7 copy.17
  69.9 0.7 copy.18
Async XLA Ops:
  0.6 1.0 %copy-start = (bf16[128,1024]{1,0:T(8,128)(2,1)S(1)}, bf16[128,1024]{1,0:T(8,128)(2,1)}, u32[]{:S(2)}) copy-start(bf16[128,1024]{1,0:T(8,128)(2,1)} %x_ref.1) | copy-start | bytes 786436
  1.6 0.9 %copy-start.1 = (bf16[128,512]{1,0:T(8,128)(2,1)S(1)}, bf16[128,512]{1,0:T(8,128)(2,1)}, u32[]{:S(2)}) copy-start(bf16[128,512]{1,0:T(8,128)(2,1)} %q_ref.1) | copy-start | bytes 393220
  2.5 0.9 %copy-start.2 = (bf16[128,512]{1,0:T(8,128)(2,1)S(1)}, bf16[128,512]{1,0:T(8,128)(2,1)}, u32[]{:S(2)}) copy-start(bf16[128,512]{1,0:T(8,128)(2,1)} %k_ref.1) | copy-start | bytes 393220
  3.4 0.9 %copy-start.3 = (bf16[128,512]{1,0:T(8,128)(2,1)S(1)}, bf16[128,512]{1,0:T(8,128)(2,1)}, u32[]{:S(2)}) copy-start(bf16[128,512]{1,0:T(8,128)(2,1)} %v_ref.1) | copy-start | bytes 393220
  4.3 0.9 %copy-start.4 = (bf16[128,512]{1,0:T(8,128)(2,1)S(1)}, bf16[128,512]{1,0:T(8,128)(2,1)}, u32[]{:S(2)}) copy-start(bf16[128,512]{1,0:T(8,128)(2,1)} %c_ref.1) | copy-start | bytes 393220
  5.2 0.8 %copy-start.5 = (s32[8,64,12]{1,0,2:T(8,128)S(1)}, s32[8,64,12]{1,0,2:T(8,128)}, u32[]{:S(2)}) copy-start(s32[8,64,12]{1,0,2:T(8,128)} %param.12) | copy-start | bytes 73732
  6.0 0.7 copy-start.6

commit v3 on v2

--- a/solution.py
+++ b/solution.py
@@ -20,9 +20,9 @@
 
 
 def kernel(
-    n, tp, g, q_ref, k_ref, v_ref, c_ref, lse_ref, pick_ref, x_ref,
+    n, tp, g, q_in, k_in, v_in, c_in, lse_in, pick_in, x_in,
     gq_ref, gk_ref, gv_ref, gw_ref,
-    bias, hot, kvs, kvt, dkvs, dkvr, gko, gvo, xs, xr, dqr, gs, gr,
+    q_ref, k_ref, v_ref, c_ref, lse_ref, pick_ref, x_ref, insem, bias, hot, kvs, kvt, dkvs, dkvr, gko, gvo, xs, xr, dqr, gs, gr,
     ssem, rsem, xssem, xrsem, dssem, drsem, gssem, grsem,
 ):
     r = n // g
@@ -38,6 +38,14 @@
     z, j = me // g, lax.rem(me, g)
     rows = n * BLK
 
+    loads = {}
+    for i, (a, b) in enumerate((
+        (pick_in, pick_ref), (k_in, k_ref), (v_in, v_ref), (x_in, x_ref),
+        (q_in, q_ref), (c_in, c_ref), (lse_in, lse_ref),
+    )):
+        loads[i] = pltpu.make_async_copy(a, b, insem.at[i])
+        loads[i].start()
+
     def iota(shape, dim):
         return lax.broadcasted_iota(jnp.int32, shape, dim)
 
@@ -75,7 +83,7 @@
 
     def each_x(fn):
         def step(i):
-            p, t2 = i // tp, lax.rem(i, tp)
+            p, t2 = lax.rem(j + i // tp, g), lax.rem(i, tp)
 
             @pl.when((p != j) | (t2 != t))
             def _():
@@ -85,6 +93,7 @@
     pool = (iota((blocks, n), 0) // bd == iota((blocks, n), 1)).astype(BF16)
     spread = (iota((heads, cols), 1) // HD == iota((heads, cols), 0)).astype(BF16)
     later = iota((n, cols), 0) > me
+    loads[0].wait()
     for b in range(bd):
         hit = jnp.zeros((heads, blocks), jnp.bool_)
         for s in range(sel):
@@ -103,15 +112,30 @@
 
     def send_kv(h):
         def step(i):
-            d = n - 1 - i
-            kvs[h, d, 0] = picked(k_ref, d, h * wide)
-            kvs[h, d, 1] = picked(v_ref, d, h * wide)
-            kv_copy(h, d, me).start()
-        each(0, n - 1 - me, step)
-
+            d = (r - 1 - i // g) * g + lax.rem(j + lax.rem(i, g), g)
+
+            @pl.when(d > me)
+            def _():
+                kvs[h, d, 0] = picked(k_ref, d, h * wide)
+                kvs[h, d, 1] = picked(v_ref, d, h * wide)
+                kv_copy(h, d, me).start()
+        each(0, (r - z) * g, step)
+
+    def send_back(h):
+        def step(i):
+            o = (i // g) * g + lax.rem(j + lax.rem(i, g), g)
+
+            @pl.when(o < me)
+            def _():
+                back_copy(h, o, me).start()
+        each(0, (z + 1) * g, step)
+
+    loads[1].wait()
+    loads[2].wait()
     for h in range(pairs):
         send_kv(h)
 
+    loads[3].wait()
     for p in range(g):
         for zl in range(rt):
             at = (zl * g + p) * w
@@ -131,6 +155,8 @@
     ids = (ids + 0.5).astype(jnp.int32).reshape(sel, heads, tok)
     ids = jnp.where(ids < me * bd + iota(ids.shape, 2) // BLK, ids, n * bd)
     owner = ids // bd
+    for i in (4, 5, 6):
+        loads[i].wait()
     less = -lse_ref[...]
 
     def put(row, need):
@@ -186,7 +212,7 @@
         dkvs[h, :, 0] = (dot(dst, qs, 1, 0) * scale).astype(BF16).reshape(n, BLK, wide)
         for i in range(1, g):
             dq_copy(h, lax.rem(j + i, g), j).start()
-        each(0, me, lambda o: back_copy(h, o, me).start())
+        send_back(h)
         gko[:, c : c + wide] = dot(dso, qs, 1, 0) * scale
 
     def weight(h):
@@ -236,6 +262,15 @@
     each_x(lambda p, t2: x_copy(p, t2, j, t).wait_send())
 
 
+def write_out(*refs):
+    sems = refs[8]
+    copies = [pltpu.make_async_copy(refs[i], refs[4 + i], sems.at[i]) for i in range(4)]
+    for copy in copies:
+        copy.start()
+    for copy in copies:
+        copy.wait()
+
+
 def body(n, tp, g, queries, keys, values, cotangent, log_sum, chosen, normed_input):
     tok, cols = queries.shape
     wide = 2 * HD
@@ -246,7 +281,11 @@
     tiles = pltpu.VMEM((pairs, n, 2, BLK, wide), BF16)
     vmem = pl.BlockSpec(memory_space=pltpu.VMEM)
     sem = pltpu.SemaphoreType.DMA
-    return pl.pallas_call(
+    hbm = pl.BlockSpec(memory_space=pltpu.HBM)
+    picks = chosen.transpose(2, 0, 1)
+    held = [pltpu.VMEM(a.shape, a.dtype) for a in (
+        queries, keys, values, cotangent, log_sum, picks, normed_input)]
+    made = pl.pallas_call(
         functools.partial(kernel, n, tp, g),
         out_shape=[
             jax.ShapeDtypeStruct((tok, cols), BF16),
@@ -254,9 +293,10 @@
             jax.ShapeDtypeStruct((tok, cols), BF16),
             jax.ShapeDtypeStruct((w, cols), F32),
         ],
-        in_specs=[vmem] * 7,
+        in_specs=[hbm] * 7,
         out_specs=[vmem] * 4,
-        scratch_shapes=[
+        scratch_shapes=held + [
+            sem((7,)),
             pltpu.VMEM((pairs, n + bd + 1, 1, 2 * tok), F32),
             pltpu.VMEM((n, bd, cols), F32),
             tiles, tiles, tiles, tiles,
@@ -272,8 +312,15 @@
             sem((pairs, g)), sem((pairs, g)),
             sem((pairs, r)), sem((pairs, r)),
         ],
-        compiler_params=pltpu.CompilerParams(has_side_effects=True, vmem_limit_bytes=48 * 1024 * 1024),
-    )(queries, keys, values, cotangent, log_sum, chosen.transpose(2, 0, 1), normed_input)
+        compiler_params=pltpu.CompilerParams(has_side_effects=True, vmem_limit_bytes=67043328),
+    )(queries, keys, values, cotangent, log_sum, picks, normed_input)
+    return pl.pallas_call(
+        write_out,
+        out_shape=[jax.ShapeDtypeStruct(a.shape, a.dtype) for a in made],
+        in_specs=[vmem] * 4,
+        out_specs=[hbm] * 4,
+        scratch_shapes=[sem((4,))],
+    )(*made)
 
 
 def solution(mesh):

time: 70.9 us -> 66.2 us (0.934)
  local copies, waits for them, and re-layouts: 8.71 us -> 0 us
  Pallas kernels: 61.3 us -> 65.4 us
    unnamed x18 -> x0, local copies, waits for them, and re-layouts: 8.71 us -> none
    pallas_call x1, Pallas kernels: 61.3 us -> 63.4 us  [body(): pl.pallas_call(functools.partial(kernel, n, tp, g), out_shape=[jax.ShapeD...]
    pallas_call x0 -> x1, Pallas kernels: none -> 2.01 us  [body(): pl.pallas_call(write_out, out_shape=[jax.ShapeDtypeStruct(a.shape, a.dtyp...]
where the time goes in v3:
time: 66.2 us; the launch traced here: 66.1 us
  Pallas kernels  65.4 us (99%)
    pallas_call x1, Pallas kernels, body(): pl.pallas_call(functools.partial(kernel, n, tp, g), out_shape=[jax.ShapeD...  63.4 us
    pallas_call x1, Pallas kernels, body(): pl.pallas_call(write_out, out_shape=[jax.ShapeDtypeStruct(a.shape, a.dtyp...  2.01 us

profile of v3, /device:TPU:0, one launch (start us, length us, event | category | flops | bytes accessed | tf_op | source)
XLA Modules:
  0.0 66.1 jit_solution(64909940572202118)
XLA Ops:
  0.6 63.4 %shard_map.102 = (bf16[128,512]{1,0:T(8,128)(2,1)}, bf16[128,512]{1,0:T(8,128)(2,1)}, bf16[128,512]{1,0:T(8,128)(2,1)}, f32[128,512]{1,0:T(8,128)}) custom-call(bf16[128,512]{1,0:T(8,128)(2,1)} %q_in.1, bf16[128,512]{1,0:T(8,128)(2,1)} %k_in.1, bf16[128,512]{1,0:T(8,128)(2,1)} %v_in.1, bf16[128,512]{1,0:T(8,128)(2,1)} %c_in.1, f32[8,128]{1,0:T(8,128)} %lse_in.1, ...), custom_call_target="tpu_custom_call" | custom-call | tf_op jit(solution)/shard_map/pallas_call | solution.py:288
  64.1 2.0 %shard_map.103 = (bf16[128,512]{1,0:T(8,128)(2,1)}, bf16[128,512]{1,0:T(8,128)(2,1)}, bf16[128,512]{1,0:T(8,128)(2,1)}, f32[128,512]{1,0:T(8,128)}) custom-call(bf16[128,512]{1,0:T(8,128)(2,1)} %get-tuple-element.8.refs_0_, bf16[128,512]{1,0:T(8,128)(2,1)} %get-tuple-element.9.refs_1_, bf16[128,512]{1,0:T(8,128)(2,1)} %get-tuple-element.10.refs_2_, ...), custom_call_target="tpu_custom_call" | custom-call | tf_op jit(solution)/shard_map/pallas_call | solution.py:317
